TPU v7x, 32 devices: a whole 2x2x4 slice. The times are simulated.
32 devices in a mesh: sp: 4 (over x, core), dp: 8 (over z, y).
Axes of the slice: x: 2, y: 2, z: 4, core: 2. Of those that a mesh axis runs over, the one named last changes fastest.
Arguments:
- tokens: bfloat16 [8, 1536, 2048], P('dp', 'sp'), may hold values from -6 to 6
- w_value: bfloat16 [2048, 1024], P('dp'), may hold values from -0.125 to 0.125
- w_gate: bfloat16 [2048, 1024], P('dp'), may hold values from -0.125 to 0.125
- conv_taps: bfloat16 [31, 1024], replicated, may hold values from -1 to 1
- norm_gain: bfloat16 [1024], replicated, may hold values from 0.099609375 to 1.8984375
- w_out: bfloat16 [1024, 2048], P(None, 'dp'), may hold values from -0.1875 to 0.1875
Outputs:
- mixed: bfloat16 [8, 1536, 2048], P('dp', 'sp')
All inputs are finite; a program needn't handle non-finite values.
Results may differ from a plain program's by a relative error of at most 0.013.
Values may be sent and summed in bfloat16 or wider, within the bound.
No kernel may reach another device: no remote copies, remote signals or barrier semaphores. Data moves between devices by JAX's collectives and lax.ppermute only.
A program may use at most 64 MiB of HBM per device.

v0:
```python
import jax
import jax.numpy as jnp
from jax import lax
from jax.sharding import PartitionSpec as P

EPSILON = 1e-06


def passed_along(x, axis, by):
    length = lax.axis_size(axis)
    pairs = [(i, i + by) for i in range(length) if 0 <= i + by < length]
    return lax.ppermute(x, axis, pairs)


def depthwise_conv(signal, local_taps, left_pad):
    kernel_form = jnp.transpose(local_taps)[:, None, :]
    result = lax.conv_general_dilated(
        signal[None],
        kernel_form,
        (1,),
        [(left_pad, 0)],
        dimension_numbers=("NCH", "OIH", "NCH"),
        feature_group_count=signal.shape[0],
        preferred_element_type=jnp.float32,
    )
    return result[0].astype(jnp.bfloat16)


def body(tokens, w_value, w_gate, conv_taps, norm_gain, w_out):
    seq_rows = tokens[0]
    tok_count = seq_rows.shape[0]
    kernel_len = conv_taps.shape[0]
    value_sum = jnp.einsum(
        "dc,td->ct",
        lax.all_gather(w_value, "dp", axis=0, tiled=True),
        seq_rows,
        preferred_element_type=jnp.float32,
    )
    gate_sum = jnp.einsum(
        "dc,td->ct",
        lax.all_gather(w_gate, "dp", axis=0, tiled=True),
        seq_rows,
        preferred_element_type=jnp.float32,
    )
    gated = (value_sum * jax.nn.sigmoid(gate_sum)).astype(jnp.bfloat16)
    last_rows = gated[:, tok_count - (kernel_len - 1) :]
    earlier = passed_along(last_rows, "sp", 1)
    extended = jnp.concatenate([earlier, gated], axis=1)
    conv_out = depthwise_conv(extended, conv_taps, 0)
    wide = conv_out.astype(jnp.float32)
    chan_mean = jnp.mean(wide, 0, keepdims=True)
    centred = wide - chan_mean
    chan_var = jnp.mean(centred * centred, 0, keepdims=True)
    normed = centred * lax.rsqrt(chan_var + EPSILON) * norm_gain.astype(jnp.float32)[:, None]
    activated = (normed * jax.nn.sigmoid(normed)).astype(jnp.bfloat16)
    projected = jnp.einsum(
        "ct,cd->td",
        activated,
        lax.all_gather(w_out, "dp", axis=1, tiled=True),
        preferred_element_type=jnp.float32,
    ).astype(jnp.bfloat16)
    return projected[None]


def solution(mesh):
    placed = (P("dp", "sp", None), P("dp", None), P("dp", None), P(), P(), P(None, "dp"))
    return jax.shard_map(
        body, mesh=mesh, in_specs=placed, out_specs=P("dp", "sp", None), check_vma=False
    )
```

profile of v0, /device:TPU:0, one launch (start us, length us, event | category | flops | bytes accessed | tf_op | source)
XLA Modules:
  0.0 246.4 jit_solution(6799378059922831921)
XLA Ops:
  6.5 0.7 all-gather.6.cloned.1.call-update
  7.3 0.0 all-gather.4.cloned.1.call-start
  7.3 0.7 all-gather.4.cloned.1.call-update
  8.0 0.0 all-gather.8.cloned.1.call-start
  8.1 0.7 all-gather.8.cloned.1.call-update
  8.7 76.3 %all-gather.6.cloned.1.call-done = bf16[2048,1024]{1,0:T(8,128)(2,1)} async-done(((bf16[256,1024]{1,0:T(8,128)(2,1)}), bf16[2048,1024]{1,0:T(8,128)(2,1)}) %all-gather.6.cloned.1.call-update) | async-done | bytes 4194320 | tf_op jit(solution)/shard_map/all_gather | solution.py:41
  85.0 4.0 %fusion.4 = f32[1024,384]{0,1:T(8,128)S(1)} fusion(bf16[2048,1024]{1,0:T(8,128)(2,1)} %all-gather.6.cloned.1.call-done, bf16[1,384,2048]{2,1,0:T(8,128)(2,1)S(1)} %copy-done), kind=kOutput, calls=%fused_computation.8 | convolution fusion | flops 1610612736 | bytes 7340032 | tf_op jit(solution)/shard_map/dc,td->ct/dot_general | solution.py:39
  89.0 69.5 %all-gather.4.cloned.1.call-done = bf16[2048,1024]{1,0:T(8,128)(2,1)} async-done(((bf16[256,1024]{1,0:T(8,128)(2,1)}), bf16[2048,1024]{1,0:T(8,128)(2,1)}) %all-gather.4.cloned.1.call-update) | async-done | bytes 4194320 | tf_op jit(solution)/shard_map/all_gather | solution.py:35
  158.5 4.1 %multiply_convert_fusion.1 = bf16[1024,384]{0,1:T(8,128)(2,1)S(1)} fusion(f32[1024,384]{0,1:T(8,128)S(1)} %fusion.4, bf16[2048,1024]{1,0:T(8,128)(2,1)} %all-gather.4.cloned.1.call-done, bf16[1,384,2048]{2,1,0:T(8,128)(2,1)S(1)} %copy-done), kind=kOutput, calls=%fused_computation.12 | convolution fusion | flops 1612578816 | bytes 8126464 | tf_op jit(solution)/shard_map/dc,td->ct/dot_general | solution.py:33
  162.6 1.3 collective-permute-start
  163.9 0.9 collective-permute-done
  164.8 0.2 maximum_bitcast_fusion
  165.0 0.1 pad
  165.0 0.2 reshape.17
  165.2 0.5 copy.12
  165.7 0.1 slice.7
  165.8 0.2 copy-done.2
  166.0 3.8 %fusion.17 = f32[8,52,1024]{2,0,1:T(8,128)S(1)} fusion(bf16[1024,1,7,30]{0,2,3,1:T(8,128)(2,1)S(1)} %slice.7, bf16[1024,1,8,52]{0,2,3,1:T(8,128)(2,1)S(1)} %copy.12, pred[8,52]{0,1:T(8,128)(4,1)S(1)} %copy-done.3, bf16[1024,1,31]{0,2,1:T(8,128)(2,1)S(1)} %bitcast.35), kind=kOutput, calls=%fused_computation.20 | convolution fusion | flops 31719424 | bytes 3049888 | tf_op jit(solution)/shard_map/conv_general_dilated | solution.py:17
  169.8 2.2 copy.14
  172.1 1.6 reshape.21
  173.7 0.2 slice_reduce_fusion
  173.8 0.3 multiply_reduce_fusion
  174.1 60.3 %all-gather.8.cloned.1.call-done = bf16[1024,2048]{1,0:T(8,128)(2,1)} async-done(((bf16[1024,256]{1,0:T(8,128)(2,1)}), bf16[1024,2048]{1,0:T(8,128)(2,1)}) %all-gather.8.cloned.1.call-update) | async-done | bytes 4194320 | tf_op jit(solution)/shard_map/all_gather | solution.py:59
  234.5 5.5 %fusion.1 = bf16[1,384,2048]{2,1,0:T(8,128)(2,1)} fusion(bf16[1024,2048]{1,0:T(8,128)(2,1)} %all-gather.8.cloned.1.call-done, f32[1,416,1024]{2,1,0:T(8,128)S(1)} %reshape.21, f32[1024]{0:T(1024)S(1)} %convert_element_type.26, f32[384]{0:T(512)S(1)} %add_rsqrt_fusion, f32[384]{0:T(512)S(1)} %broadcast_multiply_fusion), kind=kOutput, calls=%fused_computation.3 | convolution fusion | flops 1614544896 | bytes 7348224 | tf_op jit(solution)/shard_map/ct,cd->td/dot_general | solution.py:56
  (12 shorter events, 0.1 us)
Async XLA Ops:
  6.5 78.5 %copy-start = (bf16[1,384,2048]{2,1,0:T(8,128)(2,1)S(1)}, bf16[1,384,2048]{2,1,0:T(8,128)(2,1)}, u32[]{:S(2)}) copy-start(bf16[1,384,2048]{2,1,0:T(8,128)(2,1)} %param.6) | copy-start | bytes 4718596
  6.5 78.5 %all-gather.6.cloned.1.call-start = ((), (), s32[]{:S(2)}) async-start(), calls=%async_computation.1 | async-start | bytes 4718592 | tf_op jit(solution)/shard_map/all_gather | solution.py:41
  7.3 151.2 %all-gather.4.cloned.1.call-start = ((), (), s32[]{:S(2)}) async-start(), calls=%async_computation | async-start | bytes 4718592 | tf_op jit(solution)/shard_map/all_gather | solution.py:35
  8.0 226.4 %all-gather.8.cloned.1.call-start = ((), (), s32[]{:S(2)}) async-start(), calls=%async_computation.2 | async-start | bytes 4718592 | tf_op jit(solution)/shard_map/all_gather | solution.py:59
  89.0 74.9 %copy-start.1 = (bf16[1024]{0:T(1024)(128)(2,1)S(1)}, bf16[1024]{0:T(1024)(128)(2,1)}, u32[]{:S(2)}) copy-start(bf16[1024]{0:T(1024)(128)(2,1)} %param.10) | copy-start | bytes 6148
  162.6 2.2 collective-permute-start
  165.2 0.8 copy-start.2
  165.2 0.8 copy-start.3
Sparse Core Ops, SparseCore 0:
  9.5 75.5 all-gather.5
  87.1 71.3 all-gather.3
  160.5 73.8 all-gather.7
where the time goes:
time: 247 us; the launch traced here: 246 us
  waiting for transfers between devices  209 us (85%)
  matrix products  17.3 us (7%)
  between operations  13.2 us (5%)
  local copies, waits for them, and re-layouts  4.87 us (2%)
    all_gather x1, waiting for transfers between devices, body(): lax.all_gather(w_gate, 'dp', axis=0, tiled=True)  76.3 us
    all_gather x1, waiting for transfers between devices, body(): lax.all_gather(w_value, 'dp', axis=0, tiled=True)  69.5 us
    all_gather x1, waiting for transfers between devices, body(): lax.all_gather(w_out, 'dp', axis=1, tiled=True)  60.3 us
    dot_general x1, matrix products, body(): jnp.einsum('ct,cd->td', activated, lax.all_gather(w_out, 'dp', axis=1, ti...  5.46 us
  transfers between devices with their start and end apart: 4, of which 4 were waited for; matrix products, arithmetic and copies ran while one was open for 7% of the time, Pallas kernels for 0%

commit v1 on v0

--- a/solution.py
+++ b/solution.py
@@ -36,11 +36,33 @@
         seq_rows,
         preferred_element_type=jnp.float32,
     )
-    gate_sum = jnp.einsum(
-        "dc,td->ct",
-        lax.all_gather(w_gate, "dp", axis=0, tiled=True),
-        seq_rows,
-        preferred_element_type=jnp.float32,
+
+    def proceed_hubs_on(m, pos_dim, content):
+        r1, part_next, d_next = (lax.axis_size("dp"), lax.axis_index("dp"), m.shape[pos_dim])
+        by_rank = [(c, (c + 1) % r1) for c in range(r1)]
+        heap = [(c, (c - 1) % r1) for c in range(r1)]
+        m_next = r1 // 2
+        near = base_arr = m
+        mixed_arr = content(m, part_next * d_next)
+        t = 1
+        while t < m_next + 1:
+            near = lax.ppermute(near, "dp", by_rank)
+            if t < r1 - m_next:
+                base_arr = lax.ppermute(base_arr, "dp", perm=heap)
+                mixed_arr = mixed_arr + content(base_arr, (part_next + t) % r1 * d_next)
+            mixed_arr = mixed_arr + content(near, (part_next - t) % r1 * d_next)
+            t += 1
+        return mixed_arr
+
+    gate_sum = proceed_hubs_on(
+        w_gate,
+        0,
+        lambda shard, start: jnp.einsum(
+            "dc,td->ct",
+            shard,
+            lax.dynamic_slice_in_dim(seq_rows, start, shard.shape[0], axis=1),
+            preferred_element_type=jnp.float32,
+        ),
     )
     gated = (value_sum * jax.nn.sigmoid(gate_sum)).astype(jnp.bfloat16)
     last_rows = gated[:, tok_count - (kernel_len - 1) :]

time: 247 us -> 223 us (0.903)
  waiting for transfers between devices: 209 us -> 151 us
  starting transfers between devices: 1.37 us -> 21.6 us
  matrix products: 17.3 us -> 29.3 us
    all_gather x1 -> x0, waiting for transfers between devices: 76.3 us -> none  [body(): lax.all_gather(w_gate, 'dp', axis=0, tiled=True)]
    ppermute x0 -> x7, waiting for transfers between devices: none -> 72 us  [the longest x4 72 us: proceed_hubs_on(): near = lax.ppermute(near, 'dp', by_rank)]
    all_gather x1, waiting for transfers between devices: 69.5 us -> 21.1 us  [body(): lax.all_gather(w_value, 'dp', axis=0, tiled=True)]
    ppermute x0 -> x7, starting transfers between devices: none -> 19.7 us  [the longest x4 10.5 us: proceed_hubs_on(): near = lax.ppermute(near, 'dp', by_rank)]
    dot_general x1 -> x8, matrix products: 3.97 us -> 15.9 us  [body(): jnp.einsum('dc,td->ct', shard, lax.dynamic_slice_in_dim(seq_rows, start,...]
    all_gather x1, waiting for transfers between devices: 60.3 us -> 56.2 us  [body(): lax.all_gather(w_out, 'dp', axis=1, tiled=True)]
  transfers between devices with their start and end apart: 4 -> 10, of which waited for: 4 -> 6; matrix products, arithmetic and copies ran while one was open for 7% -> 13% of each run, Pallas kernels for 0% -> 0%
where the time goes in v1:
time: 223 us; the launch traced here: 222 us
  waiting for transfers between devices  151 us (68%)
  matrix products  29.3 us (13%)
  starting transfers between devices  21.6 us (10%)
  between operations  13.6 us (6%)
  local copies, waits for them, and re-layouts  5.65 us (3%)
    ppermute x4, waiting for transfers between devices, proceed_hubs_on(): near = lax.ppermute(near, 'dp', by_rank)  72 us
    all_gather x1, waiting for transfers between devices, body(): lax.all_gather(w_out, 'dp', axis=1, tiled=True)  56.2 us
    all_gather x1, waiting for transfers between devices, body(): lax.all_gather(w_value, 'dp', axis=0, tiled=True)  21.1 us
    dot_general x8, matrix products, body(): jnp.einsum('dc,td->ct', shard, lax.dynamic_slice_in_dim(seq_rows, start,...  15.9 us
    ppermute x4, starting transfers between devices, proceed_hubs_on(): near = lax.ppermute(near, 'dp', by_rank)  10.5 us
    ppermute x3, starting transfers between devices, proceed_hubs_on(): base_arr = lax.ppermute(base_arr, 'dp', perm=heap)  9.21 us
    dot_general x1, matrix products, body(): jnp.einsum('ct,cd->td', activated, lax.all_gather(w_out, 'dp', axis=1, ti...  5.46 us
  transfers between devices with their start and end apart: 10, of which 6 were waited for; matrix products, arithmetic and copies ran while one was open for 13% of the time, Pallas kernels for 0%

profile of v1, /device:TPU:0, one launch (start us, length us, event | category | flops | bytes accessed | tf_op | source)
XLA Modules:
  0.0 222.1 jit_solution(1190437085670845615)
XLA Ops:
  8.0 3.0 %collective-permute-start.1 = (bf16[256,1024]{1,0:T(8,128)(2,1)}, bf16[256,1024]{1,0:T(8,128)(2,1)}, u32[]{:S(2)}, u32[]{:S(2)}) collective-permute-start(bf16[256,1024]{1,0:T(8,128)(2,1)} %param.8), channel_id=1, source_target_pairs={{0,1},{1,2},{2,3},{3,4},{4,5},{5,6},{6,7},{7,0},{8,9},{9,10},{10,1... | collective-permute-start | bytes 1572872 | tf_op jit(solution)/shard_map/ppermute | solution.py:49
  11.1 3.1 %collective-permute-start = (bf16[256,1024]{1,0:T(8,128)(2,1)}, bf16[256,1024]{1,0:T(8,128)(2,1)}, u32[]{:S(2)}, u32[]{:S(2)}) collective-permute-start(bf16[256,1024]{1,0:T(8,128)(2,1)} %param.8), channel_id=1, source_target_pairs={{0,7},{1,0},{2,1},{3,2},{4,3},{5,4},{6,5},{7,6},{8,15},{9,8},{10,9... | collective-permute-start | bytes 1572872 | tf_op jit(solution)/shard_map/ppermute | solution.py:51
  15.6 23.8 %collective-permute-done.1 = bf16[256,1024]{1,0:T(8,128)(2,1)} collective-permute-done((bf16[256,1024]{1,0:T(8,128)(2,1)}, bf16[256,1024]{1,0:T(8,128)(2,1)}, u32[]{:S(2)}, u32[]{:S(2)}) %collective-permute-start.1) | collective-permute-done | bytes 524320 | tf_op jit(solution)/shard_map/ppermute | solution.py:49
  39.4 2.5 %collective-permute-start.3 = (bf16[256,1024]{1,0:T(8,128)(2,1)}, bf16[256,1024]{1,0:T(8,128)(2,1)S(1)}, u32[]{:S(2)}, u32[]{:S(2)}) collective-permute-start(bf16[256,1024]{1,0:T(8,128)(2,1)} %collective-permute-done.1), channel_id=1, source_target_pairs={{0,1},{1,2},{2,3},{3,4},{4,5},{5,6},{6,7},{7,0},{8,9},{9,10},{10,1... | collective-permute-start | bytes 1572872 | tf_op jit(solution)/shard_map/ppermute | solution.py:49
  41.9 3.0 %collective-permute-start.2 = (bf16[256,1024]{1,0:T(8,128)(2,1)}, bf16[256,1024]{1,0:T(8,128)(2,1)S(1)}, u32[]{:S(2)}, u32[]{:S(2)}) collective-permute-start(bf16[256,1024]{1,0:T(8,128)(2,1)} %collective-permute-done), channel_id=1, source_target_pairs={{0,7},{1,0},{2,1},{3,2},{4,3},{5,4},{6,5},{7,6},{8,15},{9,8},{10,9... | collective-permute-start | bytes 1572872 | tf_op jit(solution)/shard_map/ppermute | solution.py:51
  44.9 2.6 %fusion.31 = f32[384,1024]{1,0:T(8,128)} fusion(bf16[256,1024]{1,0:T(8,128)(2,1)} %collective-permute-done.1, bf16[1,384,2048]{2,1,0:T(8,128)(2,1)S(1)} %copy-done, s32[]{:T(128)S(6)} %select_n.59), kind=kOutput, calls=%fused_computation.35 | convolution fusion | flops 201326592 | bytes 2293764 | tf_op jit(solution)/shard_map/dc,td->ct/dot_general | solution.py:60
  47.6 2.6 %fusion.33 = f32[384,1024]{1,0:T(8,128)} fusion(bf16[256,1024]{1,0:T(8,128)(2,1)} %collective-permute-done, bf16[1,384,2048]{2,1,0:T(8,128)(2,1)S(1)} %copy-done, s32[]{:T(128)S(6)} %select_n.57), kind=kOutput, calls=%fused_computation.37 | convolution fusion | flops 201326592 | bytes 2293764 | tf_op jit(solution)/shard_map/dc,td->ct/dot_general | solution.py:60
  50.1 21.8 %collective-permute-done.3 = bf16[256,1024]{1,0:T(8,128)(2,1)S(1)} collective-permute-done((bf16[256,1024]{1,0:T(8,128)(2,1)}, bf16[256,1024]{1,0:T(8,128)(2,1)S(1)}, u32[]{:S(2)}, u32[]{:S(2)}) %collective-permute-start.3) | collective-permute-done | bytes 524320 | tf_op jit(solution)/shard_map/ppermute | solution.py:49
  71.9 2.4 %collective-permute-start.5 = (bf16[256,1024]{1,0:T(8,128)(2,1)S(1)}, bf16[256,1024]{1,0:T(8,128)(2,1)}, u32[]{:S(2)}, u32[]{:S(2)}) collective-permute-start(bf16[256,1024]{1,0:T(8,128)(2,1)S(1)} %collective-permute-done.3), channel_id=1, source_target_pairs={{0,1},{1,2},{2,3},{3,4},{4,5},{5,6},{6,7},{7,0},{8,9},{9,10},{10,1... | collective-permute-start | bytes 1572872 | tf_op jit(solution)/shard_map/ppermute | solution.py:49
  74.3 3.1 %collective-permute-start.4 = (bf16[256,1024]{1,0:T(8,128)(2,1)S(1)}, bf16[256,1024]{1,0:T(8,128)(2,1)S(1)}, u32[]{:S(2)}, u32[]{:S(2)}) collective-permute-start(bf16[256,1024]{1,0:T(8,128)(2,1)S(1)} %collective-permute-done.2), channel_id=1, source_target_pairs={{0,7},{1,0},{2,1},{3,2},{4,3},{5,4},{6,5},{7,6},{8,15},{9,8},{10,9... | collective-permute-start | bytes 1572872 | tf_op jit(solution)/shard_map/ppermute | solution.py:51
  77.4 1.6 fusion.27
  80.5 26.4 %collective-permute-done.5 = bf16[256,1024]{1,0:T(8,128)(2,1)} collective-permute-done((bf16[256,1024]{1,0:T(8,128)(2,1)S(1)}, bf16[256,1024]{1,0:T(8,128)(2,1)}, u32[]{:S(2)}, u32[]{:S(2)}) %collective-permute-start.5) | collective-permute-done | bytes 524320 | tf_op jit(solution)/shard_map/ppermute | solution.py:49
  106.9 2.6 %collective-permute-start.6 = (bf16[256,1024]{1,0:T(8,128)(2,1)}, bf16[256,1024]{1,0:T(8,128)(2,1)}, u32[]{:S(2)}, u32[]{:S(2)}) collective-permute-start(bf16[256,1024]{1,0:T(8,128)(2,1)} %collective-permute-done.5), channel_id=1, source_target_pairs={{0,1},{1,2},{2,3},{3,4},{4,5},{5,6},{6,7},{7,0},{8,9},{9,10},{10,1... | collective-permute-start | bytes 1572872 | tf_op jit(solution)/shard_map/ppermute | solution.py:49
  109.5 2.6 %fusion.23 = f32[384,1024]{1,0:T(8,128)} fusion(bf16[256,1024]{1,0:T(8,128)(2,1)} %collective-permute-done.5, bf16[1,384,2048]{2,1,0:T(8,128)(2,1)S(1)} %copy-done, s32[]{:T(128)S(6)} %select_n.67), kind=kOutput, calls=%fused_computation.27 | convolution fusion | flops 201326592 | bytes 2293764 | tf_op jit(solution)/shard_map/dc,td->ct/dot_general | solution.py:60
  112.1 1.5 fusion.25
  113.7 21.1 %all-gather.3.cloned.1.call-done = bf16[2048,1024]{1,0:T(8,128)(2,1)} async-done(((bf16[256,1024]{1,0:T(8,128)(2,1)}), bf16[2048,1024]{1,0:T(8,128)(2,1)}) %all-gather.3.cloned.1.call-update) | async-done | bytes 4194320 | tf_op jit(solution)/shard_map/all_gather | solution.py:35
  134.7 4.1 %fusion.3 = f32[1024,384]{0,1:T(8,128)S(1)} fusion(bf16[2048,1024]{1,0:T(8,128)(2,1)} %all-gather.3.cloned.1.call-done, bf16[1,384,2048]{2,1,0:T(8,128)(2,1)S(1)} %copy-done), kind=kOutput, calls=%fused_computation.8 | convolution fusion | flops 1610612736 | bytes 7340032 | tf_op jit(solution)/shard_map/dc,td->ct/dot_general | solution.py:33
  139.7 2.0 fusion.2
  141.7 1.8 collective-permute-start.7
  145.5 3.8 %fusion.14 = f32[8,52,1024]{2,0,1:T(8,128)S(1)} fusion(bf16[1024,1,7,30]{0,2,3,1:T(8,128)(2,1)S(1)} %slice.7, bf16[1024,1,8,52]{0,2,3,1:T(8,128)(2,1)S(1)} %copy.11, pred[8,52]{0,1:T(8,128)(4,1)S(1)} %copy-done.9, bf16[1024,1,31]{0,2,1:T(8,128)(2,1)S(1)} %bitcast.66), kind=kOutput, calls=%fused_computation.19 | convolution fusion | flops 31719424 | bytes 3049888 | tf_op jit(solution)/shard_map/conv_general_dilated | solution.py:17
  149.3 2.2 %copy.13 = f32[8,52,1024]{2,1,0:T(8,128)} copy(f32[8,52,1024]{2,0,1:T(8,128)S(1)} %fusion.14) | data formatting | bytes 3407872 | tf_op jit(solution)/shard_map/convert_element_type | solution.py:72
  151.6 1.6 reshape.29
  153.6 56.2 %all-gather.5.cloned.1.call-done = bf16[1024,2048]{1,0:T(8,128)(2,1)} async-done(((bf16[1024,256]{1,0:T(8,128)(2,1)}), bf16[1024,2048]{1,0:T(8,128)(2,1)}) %all-gather.5.cloned.1.call-update) | async-done | bytes 4194320 | tf_op jit(solution)/shard_map/all_gather | solution.py:81
  209.8 5.5 %fusion.1 = bf16[1,384,2048]{2,1,0:T(8,128)(2,1)} fusion(bf16[1024,2048]{1,0:T(8,128)(2,1)} %all-gather.5.cloned.1.call-done, f32[1,416,1024]{2,1,0:T(8,128)S(1)} %reshape.29, f32[1024]{0:T(1024)S(1)} %convert_element_type.26, f32[384]{0:T(512)S(1)} %add_rsqrt_fusion, f32[384]{0:T(512)S(1)} %broadcast_multiply_fusion), kind=kOutput, calls=%fused_computation.3 | convolution fusion | flops 1614544896 | bytes 7348224 | tf_op jit(solution)/shard_map/ct,cd->td/dot_general | solution.py:78
  (42 shorter events, 7.6 us)
Async XLA Ops:
  6.5 7.6 %copy-start = (bf16[1,384,2048]{2,1,0:T(8,128)(2,1)S(1)}, bf16[1,384,2048]{2,1,0:T(8,128)(2,1)}, u32[]{:S(2)}) copy-start(bf16[1,384,2048]{2,1,0:T(8,128)(2,1)} %param.6) | copy-start | bytes 4718596
  6.5 128.2 %all-gather.3.cloned.1.call-start = ((), (), s32[]{:S(2)}) async-start(), calls=%async_computation | async-start | bytes 4718592 | tf_op jit(solution)/shard_map/all_gather | solution.py:35
  7.3 202.5 %all-gather.5.cloned.1.call-start = ((), (), s32[]{:S(2)}) async-start(), calls=%async_computation.1 | async-start | bytes 4718592 | tf_op jit(solution)/shard_map/all_gather | solution.py:81
  8.0 31.4 %collective-permute-start.1 = (bf16[256,1024]{1,0:T(8,128)(2,1)}, bf16[256,1024]{1,0:T(8,128)(2,1)}, u32[]{:S(2)}, u32[]{:S(2)}) collective-permute-start(bf16[256,1024]{1,0:T(8,128)(2,1)} %param.8), channel_id=1, source_target_pairs={{0,1},{1,2},{2,3},{3,4},{4,5},{5,6},{6,7},{7,0},{8,9},{9,10},{10,1... | collective-permute-start | bytes 1572872 | tf_op jit(solution)/shard_map/ppermute | solution.py:49
  11.1 30.8 %collective-permute-start = (bf16[256,1024]{1,0:T(8,128)(2,1)}, bf16[256,1024]{1,0:T(8,128)(2,1)}, u32[]{:S(2)}, u32[]{:S(2)}) collective-permute-start(bf16[256,1024]{1,0:T(8,128)(2,1)} %param.8), channel_id=1, source_target_pairs={{0,7},{1,0},{2,1},{3,2},{4,3},{5,4},{6,5},{7,6},{8,15},{9,8},{10,9... | collective-permute-start | bytes 1572872 | tf_op jit(solution)/shard_map/ppermute | solution.py:51
  39.4 32.5 %collective-permute-start.3 = (bf16[256,1024]{1,0:T(8,128)(2,1)}, bf16[256,1024]{1,0:T(8,128)(2,1)S(1)}, u32[]{:S(2)}, u32[]{:S(2)}) collective-permute-start(bf16[256,1024]{1,0:T(8,128)(2,1)} %collective-permute-done.1), channel_id=1, source_target_pairs={{0,1},{1,2},{2,3},{3,4},{4,5},{5,6},{6,7},{7,0},{8,9},{9,10},{10,1... | collective-permute-start | bytes 1572872 | tf_op jit(solution)/shard_map/ppermute | solution.py:49
  41.9 32.4 %collective-permute-start.2 = (bf16[256,1024]{1,0:T(8,128)(2,1)}, bf16[256,1024]{1,0:T(8,128)(2,1)S(1)}, u32[]{:S(2)}, u32[]{:S(2)}) collective-permute-start(bf16[256,1024]{1,0:T(8,128)(2,1)} %collective-permute-done), channel_id=1, source_target_pairs={{0,7},{1,0},{2,1},{3,2},{4,3},{5,4},{6,5},{7,6},{8,15},{9,8},{10,9... | collective-permute-start | bytes 1572872 | tf_op jit(solution)/shard_map/ppermute | solution.py:51
  71.9 35.0 %collective-permute-start.5 = (bf16[256,1024]{1,0:T(8,128)(2,1)S(1)}, bf16[256,1024]{1,0:T(8,128)(2,1)}, u32[]{:S(2)}, u32[]{:S(2)}) collective-permute-start(bf16[256,1024]{1,0:T(8,128)(2,1)S(1)} %collective-permute-done.3), channel_id=1, source_target_pairs={{0,1},{1,2},{2,3},{3,4},{4,5},{5,6},{6,7},{7,0},{8,9},{9,10},{10,1... | collective-permute-start | bytes 1572872 | tf_op jit(solution)/shard_map/ppermute | solution.py:49
  74.3 37.8 %collective-permute-start.4 = (bf16[256,1024]{1,0:T(8,128)(2,1)S(1)}, bf16[256,1024]{1,0:T(8,128)(2,1)S(1)}, u32[]{:S(2)}, u32[]{:S(2)}) collective-permute-start(bf16[256,1024]{1,0:T(8,128)(2,1)S(1)} %collective-permute-done.2), channel_id=1, source_target_pairs={{0,7},{1,0},{2,1},{3,2},{4,3},{5,4},{6,5},{7,6},{8,15},{9,8},{10,9... | collective-permute-start | bytes 1572872 | tf_op jit(solution)/shard_map/ppermute | solution.py:51
  106.9 31.9 %collective-permute-start.6 = (bf16[256,1024]{1,0:T(8,128)(2,1)}, bf16[256,1024]{1,0:T(8,128)(2,1)}, u32[]{:S(2)}, u32[]{:S(2)}) collective-permute-start(bf16[256,1024]{1,0:T(8,128)(2,1)} %collective-permute-done.5), channel_id=1, source_target_pairs={{0,1},{1,2},{2,3},{3,4},{4,5},{5,6},{6,7},{7,0},{8,9},{9,10},{10,1... | collective-permute-start | bytes 1572872 | tf_op jit(solution)/shard_map/ppermute | solution.py:49
  134.7 4.2 %copy-start.1 = (f32[384,1024]{1,0:T(8,128)S(1)}, f32[384,1024]{1,0:T(8,128)}, u32[]{:S(2)}) copy-start(f32[384,1024]{1,0:T(8,128)} %fusion.31) | copy-start | bytes 4718596
  134.7 4.2 %copy-start.2 = (f32[384,1024]{1,0:T(8,128)S(1)}, f32[384,1024]{1,0:T(8,128)}, u32[]{:S(2)}) copy-start(f32[384,1024]{1,0:T(8,128)} %fusion.33) | copy-start | bytes 4718596
  134.7 4.2 %copy-start.3 = (f32[384,1024]{1,0:T(8,128)S(1)}, f32[384,1024]{1,0:T(8,128)}, u32[]{:S(2)}) copy-start(f32[384,1024]{1,0:T(8,128)} %fusion.27) | copy-start | bytes 4718596
  134.7 4.2 %copy-start.4 = (f32[384,1024]{1,0:T(8,128)S(1)}, f32[384,1024]{1,0:T(8,128)}, u32[]{:S(2)}) copy-start(f32[384,1024]{1,0:T(8,128)} %fusion.29) | copy-start | bytes 4718596
  134.7 4.5 %copy-start.5 = (f32[384,1024]{1,0:T(8,128)S(1)}, f32[384,1024]{1,0:T(8,128)}, u32[]{:S(2)}) copy-start(f32[384,1024]{1,0:T(8,128)} %fusion.23) | copy-start | bytes 4718596
  134.7 5.0 %copy-start.6 = (f32[384,1024]{1,0:T(8,128)S(1)}, f32[384,1024]{1,0:T(8,128)}, u32[]{:S(2)}) copy-start(f32[384,1024]{1,0:T(8,128)} %fusion.25) | copy-start | bytes 4718596
  138.9 4.7 %copy-start.7 = (bf16[1024]{0:T(1024)(128)(2,1)S(1)}, bf16[1024]{0:T(1024)(128)(2,1)}, u32[]{:S(2)}) copy-start(bf16[1024]{0:T(1024)(128)(2,1)} %param.10) | copy-start | bytes 6148
  141.7 2.5 %collective-permute-start.7 = (bf16[1024,30]{0,1:T(8,128)(2,1)S(1)}, bf16[1024,30]{0,1:T(8,128)(2,1)S(1)}, u32[]{:S(2)}, u32[]{:S(2)}) collective-permute-start(bf16[1024,30]{0,1:T(8,128)(2,1)S(1)} %slice.6), channel_id=1, source_target_pairs={{0,8},{8,16},{16,24},{1,9},{9,17},{17,25},{2,10},{10,18},{18,26},{... | collective-permute-start | bytes 184328 | tf_op jit(solution)/shard_map/ppermute | solution.py:12
  144.7 0.8 copy-start.8
  144.7 0.8 copy-start.9
Sparse Core Ops, SparseCore 0:
  9.5 125.2 all-gather.2
  136.8 72.9 all-gather.4
